TPU v7x, 512 devices: a whole 4x8x8 slice. The times are simulated.
512 devices in a mesh: sp: 128 (over z, y, core), tp: 4 (over x).
Axes of the slice: x: 4, y: 8, z: 8, core: 2. Of those that a mesh axis runs over, the one named last changes fastest.
Arguments:
- stream: bfloat16 [32768, 2048], P('sp', 'tp'), may hold values from -6 to 6
- norm_gain: float32 [2, 2048], replicated, may hold values from 0.1 to 1.9
- w_value: bfloat16 [2, 2048, 1024], P(None, 'sp', 'tp'), may hold values from -0.125 to 0.125
- w_gate: bfloat16 [2, 2048, 1024], P(None, 'sp', 'tp'), may hold values from -0.125 to 0.125
- conv_taps: float32 [2, 128, 1024], P(None, None, 'tp'), as said below
- channel_gain: float32 [2, 1024], P(None, 'tp'), may hold values from 0.1 to 1.9
- w_out: bfloat16 [2, 1024, 2048], P(None, 'tp', 'sp'), may hold values from -0.1875 to 0.1875
Outputs:
- result: bfloat16 [32768, 2048], P('sp', 'tp')
Inputs may be any that keep to these rules, and one draw needn't show every extreme that they name: `conv_taps`: taps of each block of 128 consecutive channels share a scale factor of its own.
All inputs are finite; a program needn't handle non-finite values.
Results may differ from a plain program's by a relative error of at most 0.012.
Values may be sent and summed in bfloat16 or wider, within the bound.
No kernel may reach another device: no remote copies, remote signals or barrier semaphores. Data moves between devices by JAX's collectives and lax.ppermute only.
A program may use at most 64 MiB of HBM per device.

v0:
```python
import jax
import jax.numpy as jnp
from jax import lax
from jax.sharding import Mesh
from jax.sharding import PartitionSpec as P

C = 1024
LAYERS = 2
SP = ("sp_0", "sp_1", "sp_2")


def laid_out(parts, dim):
    parts = jnp.moveaxis(parts, 0, dim)
    lengths = parts.shape
    return parts.reshape(*lengths[:dim], lengths[dim] * lengths[dim + 1], *lengths[dim + 2 :])


def sent_to_all(shard, axis):
    copies = jnp.broadcast_to(shard, (lax.axis_size(axis), *shard.shape))
    return lax.all_to_all(copies, axis, split_axis=0, concat_axis=0, tiled=True)


def collect(shard, axis, dim):
    return laid_out(sent_to_all(shard, axis), dim)


def in_one_piece(arrays, axis, dim, along):
    both = jnp.concatenate(arrays, axis=along)
    whole, at, done = (lax.all_gather(both, axis, axis=dim, tiled=True), 0, [])
    for a in arrays:
        done.append(lax.slice_in_dim(whole, at, at + a.shape[along], axis=along))
        at += a.shape[along]
    return tuple(done)


def from_behind(value, axis, steps):
    count = lax.axis_size(axis)
    initial, last = (max(0, -steps), min(count, count - steps))
    return lax.ppermute(value, axis, [(source, source + steps) for source in range(initial, last)])


def of_everyone(shard, axis):
    return sent_to_all(shard, axis).sum(axis=0)


def stacked_from(shard, axes, turns):
    parts = shard[None]
    for k in turns:
        parts = lax.all_gather(parts, axes[k], axis=0, tiled=True)
    held = [lax.axis_size(axes[k]) for k in reversed(turns)]
    parts = parts.reshape(*held, *shard.shape)
    turned = sorted(range(len(turns)), key=lambda place: turns[len(turns) - 1 - place])
    return parts.transpose(*turned, *range(len(turns), parts.ndim)).reshape(-1, *shard.shape)


def gathered_by_axis(shard, axes, turns, dim):
    return laid_out(stacked_from(shard, axes, turns), dim)


def split_up(shard, dim, size):
    lengths = shard.shape
    parts = shard.reshape(*lengths[:dim], size, lengths[dim] // size, *lengths[dim + 1 :])
    return jnp.moveaxis(parts, dim, 0)


def sum_at_owner(shard, axis, dim):
    parts = split_up(shard, dim, lax.axis_size(axis))
    arrived = lax.all_to_all(parts, axis, split_axis=0, concat_axis=0, tiled=True)
    return arrived.astype(jnp.float32).sum(axis=0)


def shards(stream, norm_gain, w_value, w_gate, conv_taps, channel_gain, w_out):
    x = stream
    tokens_here = stream.shape[0]
    local_ch = w_value.shape[2]
    taps = conv_taps.shape[1]
    for layer in range(LAYERS):
        whole = collect(x, "tp", 1).astype(jnp.float32)
        normed = (
            whole
            * lax.rsqrt(jnp.mean(whole * whole, axis=1, keepdims=True) + 1e-06)
            * norm_gain[layer]
        ).astype(jnp.bfloat16)
        value_whole, gate_whole = in_one_piece((w_value[layer], w_gate[layer]), SP, 0, 1)
        value = jnp.dot(normed, value_whole, preferred_element_type=jnp.float32)
        gate = jnp.dot(normed, gate_whole, preferred_element_type=jnp.float32)
        glu = (value * jax.nn.sigmoid(gate)).astype(jnp.bfloat16)
        before = from_behind(glu[tokens_here - taps :], SP, 1)
        padded = jnp.concatenate([before[1:], glu], axis=0).astype(jnp.float32)
        conv = lax.conv_general_dilated(
            padded[None],
            conv_taps[layer][:, None, :],
            (1,),
            "VALID",
            dimension_numbers=("NWC", "WIO", "NWC"),
            feature_group_count=local_ch,
            precision=lax.Precision.HIGHEST,
        )[0]
        mean = of_everyone(jnp.sum(conv, axis=1, keepdims=True), "tp") / C
        centred = conv - mean
        spread = of_everyone(jnp.sum(centred * centred, axis=1, keepdims=True), "tp") / C
        act = jax.nn.silu(centred * lax.rsqrt(spread + 1e-05) * channel_gain[layer]).astype(
            jnp.bfloat16
        )
        out_whole = gathered_by_axis(w_out[layer], (("sp_0", "sp_1"), "sp_2"), (0, 1), 1)
        terms = jnp.dot(act, out_whole, preferred_element_type=jnp.float32)
        branch = sum_at_owner(terms.astype(jnp.bfloat16), "tp", 1)
        x = (x.astype(jnp.float32) + branch).astype(jnp.bfloat16)
    return x


def solution(mesh):
    finer = Mesh(mesh.devices.reshape(8, 8, 2, mesh.shape["tp"]), ("sp_0", "sp_1", "sp_2", "tp"))
    in_specs = (
        P(SP, "tp"),
        P(),
        P(None, SP, "tp"),
        P(None, SP, "tp"),
        P(None, None, "tp"),
        P(None, "tp"),
        P(None, "tp", SP),
    )
    out_specs = P(SP, "tp")
    return jax.shard_map(
        shards, mesh=finer, in_specs=in_specs, out_specs=out_specs, check_vma=False
    )
```

profile of v0, /device:TPU:24, one launch (start us, length us, event | category | flops | bytes accessed | tf_op | source)
XLA Modules:
  0.0 303.7 jit_solution(6002797034493604324)
XLA Ops:
  8.7 60.0 %all_gather.19 = bf16[64,256,16]{1,2,0:T(8,128)(2,1)} all-gather(bf16[1,256,16]{1,2,0:T(8,128)(2,1)S(1)} %get-tuple-element.13), channel_id=1, replica_groups=mesh['sp_0'=8,'sp_1'=8,'sp_2'=2,'tp'=4] {'sp_0','sp_1'}, dimensions={0}, use_global_device_ids=true | all-gather | bytes 532480 | tf_op jit(solution)/shard_map/all_gather | solution.py:49
  70.9 4.3 %all-to-all-start = ((bf16[4,256,512]{1,2,0:T(8,128)(2,1)}), bf16[4,256,512]{1,2,0:T(8,128)(2,1)S(1)}, u32[]{:S(2)}, u32[]{:S(2)}) async-start(bf16[4,256,512]{1,2,0:T(8,128)(2,1)} %broadcast_in_dim.30), calls=%async_computation | async-start | bytes 2097152 | tf_op jit(solution)/shard_map/all_to_all | solution.py:20
  75.9 10.1 %all-to-all-done = bf16[4,256,512]{1,2,0:T(8,128)(2,1)S(1)} async-done(((bf16[4,256,512]{1,2,0:T(8,128)(2,1)}), bf16[4,256,512]{1,2,0:T(8,128)(2,1)S(1)}, u32[]{:S(2)}, u32[]{:S(2)}) %all-to-all-start) | async-done | bytes 1048608 | tf_op jit(solution)/shard_map/all_to_all | solution.py:20
  86.7 11.0 %all-gather.5.cloned.1.call-done = bf16[2048,512]{1,0:T(8,128)(2,1)} async-done(((bf16[16,512]{1,0:T(8,128)(2,1)}), bf16[2048,512]{1,0:T(8,128)(2,1)}) %all-gather.5.cloned.1.call-update) | async-done | bytes 2097168 | tf_op jit(solution)/shard_map/all_gather | solution.py:29
  97.7 1.8 fusion.18
  100.2 2.1 collective-permute-start
  102.3 3.4 %collective-permute-done = bf16[128,256]{1,0:T(8,128)(2,1)S(1)} collective-permute-done((bf16[128,256]{1,0:T(8,128)(2,1)S(1)}, bf16[128,256]{1,0:T(8,128)(2,1)S(1)}, u32[]{:S(2)}, u32[]{:S(2)}) %collective-permute-start) | collective-permute-done | bytes 65568 | tf_op jit(solution)/shard_map/ppermute | solution.py:39
  105.8 4.8 %fusion.42 = (f32[256]{0:T(256)S(1)}, f32[1,256,256]{2,0,1:T(1,128)S(1)}) fusion(f32[1,128,256]{2,1,0:T(8,128)S(1)} %get-tuple-element.6, bf16[1,383,256]{2,1,0:T(8,128)(2,1)S(1)} %maximum_bitcast_fusion), kind=kOutput, calls=%fused_computation.76 | convolution fusion | flops 100728576 | bytes 590336 | tf_op jit(solution)/shard_map/conv_general_dilated | solution.py:90
  110.7 9.2 %all_to_all.40 = f32[4,256,1]{1,2,0:T(1,128)S(1)} all-to-all(f32[4,256,1]{1,2,0:T(1,128)S(1)} %broadcast_in_dim.32), channel_id=1, replica_groups=mesh['sp_0'=8,'sp_1'=8,'sp_2'=2,'tp'=4] {'tp'}, dimensions={0} | all-to-all | bytes 8192 | tf_op jit(solution)/shard_map/all_to_all | solution.py:20
  120.7 3.2 %all-to-all-start.2 = ((f32[4,256,1]{1,2,0:T(1,128)}), f32[4,256,1]{1,2,0:T(1,128)S(1)}, u32[]{:S(2)}, u32[]{:S(2)}) async-start(f32[4,256,1]{1,2,0:T(1,128)} %broadcast_in_dim.33), calls=%async_computation.2 | async-start | bytes 8192 | tf_op jit(solution)/shard_map/all_to_all | solution.py:20
  124.1 1.4 copy.40
  125.4 3.8 %all-to-all-done.2 = f32[4,256,1]{1,2,0:T(1,128)S(1)} async-done(((f32[4,256,1]{1,2,0:T(1,128)}), f32[4,256,1]{1,2,0:T(1,128)S(1)}, u32[]{:S(2)}, u32[]{:S(2)}) %all-to-all-start.2) | async-done | bytes 4128 | tf_op jit(solution)/shard_map/all_to_all | solution.py:20
  129.9 15.3 %all_to_all.41 = bf16[4,256,512]{2,1,0:T(8,128)(2,1)S(1)} all-to-all(bf16[4,256,512]{2,1,0:T(8,128)(2,1)S(1)} %bitcast.96), channel_id=1, replica_groups=mesh['sp_0'=8,'sp_1'=8,'sp_2'=2,'tp'=4] {'tp'}, dimensions={0} | all-to-all | bytes 2097152 | tf_op jit(solution)/shard_map/all_to_all | solution.py:68
  145.6 14.3 %all_to_all.42 = bf16[4,256,512]{1,2,0:T(8,128)(2,1)S(1)} all-to-all(bf16[4,256,512]{1,2,0:T(8,128)(2,1)S(1)} %broadcast_in_dim.34), channel_id=1, replica_groups=mesh['sp_0'=8,'sp_1'=8,'sp_2'=2,'tp'=4] {'tp'}, dimensions={0} | all-to-all | bytes 2097152 | tf_op jit(solution)/shard_map/all_to_all | solution.py:20
  160.5 40.8 %all-gather.9.cloned.1.call-done = bf16[2048,512]{1,0:T(8,128)(2,1)} async-done(((bf16[16,512]{1,0:T(8,128)(2,1)}), bf16[2048,512]{1,0:T(8,128)(2,1)}) %all-gather.9.cloned.1.call-update) | async-done | bytes 2097168 | tf_op jit(solution)/shard_map/all_gather | solution.py:29
  201.3 1.8 fusion.15
  203.7 2.1 collective-permute-start.1
  205.9 52.8 %all_gather.22 = bf16[64,256,16]{1,2,0:T(8,128)(2,1)} all-gather(bf16[1,256,16]{1,2,0:T(8,128)(2,1)S(1)} %get-tuple-element.14), channel_id=1, replica_groups=mesh['sp_0'=8,'sp_1'=8,'sp_2'=2,'tp'=4] {'sp_0','sp_1'}, dimensions={0}, use_global_device_ids=true | all-gather | bytes 532480 | tf_op jit(solution)/shard_map/all_gather | solution.py:49
  258.8 4.8 %fusion.43 = (f32[256]{0:T(256)S(1)}, f32[1,256,256]{2,0,1:T(1,128)S(1)}) fusion(f32[1,128,256]{2,1,0:T(8,128)S(1)} %get-tuple-element.5, bf16[1,383,256]{2,1,0:T(8,128)(2,1)S(1)} %maximum_bitcast_fusion.1), kind=kOutput, calls=%fused_computation.77 | convolution fusion | flops 100728576 | bytes 590336 | tf_op jit(solution)/shard_map/conv_general_dilated | solution.py:90
  263.6 9.3 %all_to_all.43 = f32[4,256,1]{1,2,0:T(1,128)S(1)} all-to-all(f32[4,256,1]{1,2,0:T(1,128)S(1)} %broadcast_in_dim.36), channel_id=1, replica_groups=mesh['sp_0'=8,'sp_1'=8,'sp_2'=2,'tp'=4] {'tp'}, dimensions={0} | all-to-all | bytes 8192 | tf_op jit(solution)/shard_map/all_to_all | solution.py:20
  273.8 3.2 %all-to-all-start.6 = ((f32[4,256,1]{1,2,0:T(1,128)}), f32[4,256,1]{1,2,0:T(1,128)S(1)}, u32[]{:S(2)}, u32[]{:S(2)}) async-start(f32[4,256,1]{1,2,0:T(1,128)} %broadcast_in_dim.37), calls=%async_computation.6 | async-start | bytes 8192 | tf_op jit(solution)/shard_map/all_to_all | solution.py:20
  277.1 1.4 copy.46
  278.4 3.9 %all-to-all-done.6 = f32[4,256,1]{1,2,0:T(1,128)S(1)} async-done(((f32[4,256,1]{1,2,0:T(1,128)}), f32[4,256,1]{1,2,0:T(1,128)S(1)}, u32[]{:S(2)}, u32[]{:S(2)}) %all-to-all-start.6) | async-done | bytes 4128 | tf_op jit(solution)/shard_map/all_to_all | solution.py:20
  282.9 13.3 %all_to_all.44 = bf16[4,256,512]{2,1,0:T(8,128)(2,1)S(1)} all-to-all(bf16[4,256,512]{2,1,0:T(8,128)(2,1)S(1)} %bitcast.97), channel_id=1, replica_groups=mesh['sp_0'=8,'sp_1'=8,'sp_2'=2,'tp'=4] {'tp'}, dimensions={0} | all-to-all | bytes 2097152 | tf_op jit(solution)/shard_map/all_to_all | solution.py:68
  (70 shorter events, 12.0 us)
Async XLA Ops:
  6.5 91.2 %all-gather.5.cloned.1.call-start = ((), (), s32[]{:S(2)}) async-start(), calls=%async_computation.8 | async-start | bytes 2113536 | tf_op jit(solution)/shard_map/all_gather | solution.py:29
  7.9 116.1 %all-gather.7.cloned.1.call-start = ((), (), s32[]{:S(2)}) async-start(), calls=%async_computation.9 | async-start | bytes 1572864 | tf_op jit(solution)/shard_map/all_gather | solution.py:49
  68.7 7.2 %copy-start.4 = (f32[2,2048]{1,0:T(2,128)S(1)}, f32[2,2048]{1,0:T(2,128)}, u32[]{:S(2)}) copy-start(f32[2,2048]{1,0:T(2,128)} %param.8) | copy-start | bytes 49156
  70.9 15.2 %all-to-all-start = ((bf16[4,256,512]{1,2,0:T(8,128)(2,1)}), bf16[4,256,512]{1,2,0:T(8,128)(2,1)S(1)}, u32[]{:S(2)}, u32[]{:S(2)}) async-start(bf16[4,256,512]{1,2,0:T(8,128)(2,1)} %broadcast_in_dim.30), calls=%async_computation | async-start | bytes 2097152 | tf_op jit(solution)/shard_map/all_to_all | solution.py:20
  75.2 126.2 %all-gather.9.cloned.1.call-start = ((), (), s32[]{:S(2)}) async-start(), calls=%async_computation.10 | async-start | bytes 2113536 | tf_op jit(solution)/shard_map/all_gather | solution.py:29
  97.7 1.9 copy-start.2
  99.6 2.7 copy-start.3
  100.2 5.6 %collective-permute-start = (bf16[128,256]{1,0:T(8,128)(2,1)S(1)}, bf16[128,256]{1,0:T(8,128)(2,1)S(1)}, u32[]{:S(2)}, u32[]{:S(2)}) collective-permute-start(bf16[128,256]{1,0:T(8,128)(2,1)S(1)} %slice.82), channel_id=1, source_target_pairs={{0,4},{4,8},{8,12},{12,16},{16,20},{20,24},{24,28},{28,32},{32,36}... | collective-permute-start | bytes 196616 | tf_op jit(solution)/shard_map/ppermute | solution.py:39
  105.8 18.2 %copy-start.5 = (f32[2,256]{1,0:T(2,128)S(1)}, f32[2,256]{1,0:T(2,128)}, u32[]{:S(2)}) copy-start(f32[2,256]{1,0:T(2,128)} %param.12) | copy-start | bytes 6148
  120.7 8.5 %all-to-all-start.2 = ((f32[4,256,1]{1,2,0:T(1,128)}), f32[4,256,1]{1,2,0:T(1,128)S(1)}, u32[]{:S(2)}, u32[]{:S(2)}) async-start(f32[4,256,1]{1,2,0:T(1,128)} %broadcast_in_dim.33), calls=%async_computation.2 | async-start | bytes 8192 | tf_op jit(solution)/shard_map/all_to_all | solution.py:20
  124.0 153.1 %all-gather.11.cloned.1.call-start = ((), (), s32[]{:S(2)}) async-start(), calls=%async_computation.11 | async-start | bytes 1572864 | tf_op jit(solution)/shard_map/all_gather | solution.py:49
  129.9 15.4 %copy-start = (bf16[256,512]{1,0:T(8,128)(2,1)S(1)}, bf16[256,512]{1,0:T(8,128)(2,1)}, u32[]{:S(2)}) copy-start(bf16[256,512]{1,0:T(8,128)(2,1)} %param.7) | copy-start | bytes 786436
  201.3 1.9 copy-start.1
  203.7 54.9 %collective-permute-start.1 = (bf16[128,256]{1,0:T(8,128)(2,1)S(1)}, bf16[128,256]{1,0:T(8,128)(2,1)S(1)}, u32[]{:S(2)}, u32[]{:S(2)}) collective-permute-start(bf16[128,256]{1,0:T(8,128)(2,1)S(1)} %slice.86), channel_id=1, source_target_pairs={{0,4},{4,8},{8,12},{12,16},{16,20},{20,24},{24,28},{28,32},{32,36}... | collective-permute-start | bytes 196616 | tf_op jit(solution)/shard_map/ppermute | solution.py:39
  273.8 8.5 %all-to-all-start.6 = ((f32[4,256,1]{1,2,0:T(1,128)}), f32[4,256,1]{1,2,0:T(1,128)S(1)}, u32[]{:S(2)}, u32[]{:S(2)}) async-start(f32[4,256,1]{1,2,0:T(1,128)} %broadcast_in_dim.37), calls=%async_computation.6 | async-start | bytes 8192 | tf_op jit(solution)/shard_map/all_to_all | solution.py:20
Sparse Core Ops, SparseCore 0:
  10.5 87.2 all-gather.4
  99.8 14.3 all-gather.6
  117.3 83.9 all-gather.8
  258.8 14.8 all-gather.10
where the time goes:
time: 304 us
  blocking collectives  174 us (57%)
  waiting for transfers between devices  73.2 us (24%)
  matrix products  15.4 us (5%)
  starting transfers between devices  15.1 us (5%)
  between operations  13.4 us (4%)
  local copies, waits for them, and re-layouts  8.17 us (3%)
  other arithmetic  4.21 us (1%)
    all_gather x2, blocking collectives, stacked_from(): parts = lax.all_gather(parts, axes[k], axis=0, tiled=True)  113 us
    all_gather x2, waiting for transfers between devices, in_one_piece(): whole, at, done = (lax.all_gather(both, axis, axis=dim, tiled=True), 0, [])  51.8 us
    all_to_all x3, blocking collectives, sent_to_all(): return lax.all_to_all(copies, axis, split_axis=0, concat_axis=0, tiled=True)  32.8 us
    all_to_all x2, blocking collectives, sum_at_owner(): lax.all_to_all(parts, axis, split_axis=0, concat_axis=0, tiled=True)  28.6 us
    all_to_all x3, waiting for transfers between devices, sent_to_all(): return lax.all_to_all(copies, axis, split_axis=0, concat_axis=0, tiled=True)  17.8 us
    all_to_all x3, starting transfers between devices, sent_to_all(): return lax.all_to_all(copies, axis, split_axis=0, concat_axis=0, tiled=True)  10.8 us
    conv_general_dilated x2, matrix products, shards(): lax.conv_general_dilated(padded[None], conv_taps[layer][:, None, :], (1,)...  9.67 us
  transfers between devices with their start and end apart: 9, of which 6 were waited for; matrix products, arithmetic and copies ran while one was open for 7% of the time, Pallas kernels for 0%

commit v1 on v0

v1 whole, which is shorter than its diff:
```python
import jax
import jax.numpy as jnp
from jax import lax
from jax.sharding import Mesh
from jax.sharding import PartitionSpec as P

C = 1024
LAYERS = 2
SP = ("z", "y", "c")
BF = jnp.bfloat16
F32 = jnp.float32


def spread_copies(block, axes):
    n = lax.axis_size(axes)
    copies = jnp.broadcast_to(block, (n, *block.shape))
    return lax.all_to_all(copies, axes, split_axis=0, concat_axis=0, tiled=True)


def swap_cores(v):
    return lax.ppermute(v, "c", [(0, 1), (1, 0)])


def by_core(first, mine, other):
    return jnp.where(first, mine, other), jnp.where(first, other, mine)


def to_column_owner(v, flip):
    nz, nc, nx = lax.axis_size("z"), lax.axis_size("c"), lax.axis_size("x")
    nb = nz // nx
    pairs = []
    for z in range(nz):
        for c in range(nc):
            for x in range(nx):
                a, b = divmod(z, nb)
                to = ((x * nb + b) * nc + (c ^ flip)) * nx + a
                pairs.append(((z * nc + c) * nx + x, to))
    return lax.ppermute(v, ("z", "c", "x"), pairs)


def split_three(v):
    hi = lax.reduce_precision(v, 8, 7)
    rest = v - hi
    mid = lax.reduce_precision(rest, 8, 7)
    return jnp.stack([hi, mid, rest - mid]).astype(BF)


def shards(stream, norm_gain, w_value, w_gate, conv_taps, channel_gain, w_out):
    x = stream
    tokens = stream.shape[0]
    ch = w_value.shape[2]
    taps = conv_taps.shape[1]
    nx = lax.axis_size("x")
    first = lax.axis_index("c") == 0

    keep, send = by_core(first, w_value, w_gate)
    top, bottom = by_core(first, keep, swap_cores(send))
    half_proj = jnp.concatenate([top, bottom], axis=1)

    out_t = jnp.swapaxes(w_out, 1, 2)
    keep, send = by_core(first, out_t[:, :, : ch // 2], out_t[:, :, ch // 2 :])
    top, bottom = by_core(first, to_column_owner(keep, 0), to_column_owner(send, 1))
    half_out = jnp.concatenate([top, bottom], axis=1)

    for layer in range(LAYERS):
        proj_mine = spread_copies(half_proj[layer], ("z", "y")).reshape(-1, ch)
        proj_other = swap_cores(proj_mine)
        out_mine = spread_copies(half_out[layer], ("z", "y")).reshape(nx, -1, ch // 2)
        out_other = swap_cores(out_mine)

        whole = spread_copies(x, "x").astype(F32)
        mean_sq = jnp.sum(whole * whole, axis=(0, 2), keepdims=True) / (nx * x.shape[1])
        normed = whole * lax.rsqrt(mean_sq + 1e-06) * norm_gain[layer].reshape(nx, 1, -1)
        normed = jnp.moveaxis(normed.astype(BF), 0, 1).reshape(tokens, -1)
        a = jnp.dot(normed, proj_mine, preferred_element_type=F32)
        b = jnp.dot(normed, proj_other, preferred_element_type=F32)
        value, gate = by_core(first, a, b)
        glu = (value * jax.nn.sigmoid(gate)).astype(BF)
        count = lax.axis_size(SP)
        before = lax.ppermute(glu[tokens - taps :], SP, [(i, i + 1) for i in range(count - 1)])
        padded = jnp.concatenate([before[1:], glu], axis=0).astype(F32)
        conv = lax.conv_general_dilated(
            padded[None],
            conv_taps[layer][:, None, :],
            (1,),
            "VALID",
            dimension_numbers=("NWC", "WIO", "NWC"),
            feature_group_count=ch,
            precision=lax.Precision.HIGHEST,
        )[0]
        mean_here = jnp.mean(conv, axis=1)
        centred = (conv - mean_here[:, None]).astype(BF)
        extra = jnp.concatenate(
            [split_three(mean_here), split_three(channel_gain[layer]), jnp.zeros((10, ch), BF)]
        )
        everyone = spread_copies(jnp.concatenate([centred, extra]), "x")
        tail = everyone[:, tokens:].astype(F32)
        means = tail[:, 0] + tail[:, 1] + tail[:, 2]
        gains = tail[:, 3] + tail[:, 4] + tail[:, 5]
        shift = means - jnp.mean(means, axis=0)
        centred = everyone[:, :tokens].astype(F32) + shift[:, :, None]
        spread = jnp.sum(centred * centred, axis=(0, 2)) / C
        act = jax.nn.silu(centred * lax.rsqrt(spread + 1e-05)[None, :, None] * gains[:, None, :]).astype(BF)
        act_mine, act_other = by_core(first, act[:, :, : ch // 2], act[:, :, ch // 2 :])
        branch = jnp.einsum("ktr,knr->tn", act_mine, out_mine, preferred_element_type=F32)
        branch += jnp.einsum("ktr,knr->tn", act_other, out_other, preferred_element_type=F32)
        x = (x.astype(F32) + branch).astype(BF)
    return x


def solution(mesh):
    finer = Mesh(mesh.devices.reshape(8, 8, 2, mesh.shape["tp"]), ("z", "y", "c", "x"))
    in_specs = (
        P(SP, "x"),
        P(),
        P(None, SP, "x"),
        P(None, SP, "x"),
        P(None, None, "x"),
        P(None, "x"),
        P(None, "x", SP),
    )
    return jax.shard_map(shards, mesh=finer, in_specs=in_specs, out_specs=P(SP, "x"), check_vma=False)
```

time: 304 us -> 227 us (0.75)
  the two profiles are of different devices: /device:TPU:24 before, /device:TPU:9 now
where the time goes in v1:
time: 227 us; the launch traced here: 226 us
  waiting for transfers between devices  95.9 us (42%)
  starting transfers between devices  90.9 us (40%)
  matrix products  16.1 us (7%)
  blocking collectives  10.5 us (5%)
  local copies, waits for them, and re-layouts  7.63 us (3%)
  other arithmetic  4.64 us (2%)
    all_to_all x7, waiting for transfers between devices, spread_copies(): return lax.all_to_all(copies, axes, split_axis=0, concat_axis=0, tiled=True)  94.7 us
    all_to_all x7, starting transfers between devices, spread_copies(): return lax.all_to_all(copies, axes, split_axis=0, concat_axis=0, tiled=True)  55.4 us
    ppermute x5, starting transfers between devices, swap_cores(): return lax.ppermute(v, 'c', [(0, 1), (1, 0)])  16.9 us
    ppermute x2, starting transfers between devices, shards(): lax.ppermute(glu[tokens - taps:], SP, [(i, i + 1) for i in range(count -...  13.6 us
    all_to_all x1, blocking collectives, spread_copies(): return lax.all_to_all(copies, axes, split_axis=0, concat_axis=0, tiled=True)  10.5 us
    conv_general_dilated x2, matrix products, shards(): lax.conv_general_dilated(padded[None], conv_taps[layer][:, None, :], (1,)...  9.67 us
    broadcast_in_dim x8, local copies, waits for them, and re-layouts, spread_copies(): copies = jnp.broadcast_to(block, (n, *block.shape))  6.87 us
    ppermute x2, starting transfers between devices, to_column_owner(): return lax.ppermute(v, ('z', 'c', 'x'), pairs)  4.89 us
  transfers between devices with their start and end apart: 16, of which 9 were waited for; matrix products, arithmetic and copies ran while one was open for 8% of the time, Pallas kernels for 0%

profile of v1, /device:TPU:9, one launch (start us, length us, event | category | flops | bytes accessed | tf_op | source)
XLA Modules:
  0.0 226.2 jit_solution(7763587302457244946)
XLA Ops:
  0.7 2.6 %collective-permute-start = (bf16[2,16,256]{2,1,0:T(8,128)(2,1)S(1)}, bf16[2,16,256]{2,1,0:T(8,128)(2,1)S(1)}, u32[]{:S(2)}, u32[]{:S(2)}) collective-permute-start(bf16[2,16,256]{2,1,0:T(8,128)(2,1)S(1)} %broadcast_select_fusion.2), channel_id=1, source_target_pairs={{0,4},{4,0},{1,5},{5,1},{2,6},{6,2},{3,7},{7,3},{8,12},{12,8},{9,1... | collective-permute-start | bytes 49160 | tf_op jit(solution)/shard_map/ppermute | solution.py:21
  6.0 16.2 %all-to-all-start.1 = ((bf16[64,32,256]{2,1,0:T(8,128)(2,1)}), bf16[64,32,256]{2,1,0:T(8,128)(2,1)S(1)}, u32[]{:S(2)}, u32[]{:S(2)}) async-start(bf16[64,32,256]{2,1,0:T(8,128)(2,1)} %broadcast_in_dim.21), calls=%async_computation.1 | async-start | bytes 2097152 | tf_op jit(solution)/shard_map/all_to_all | solution.py:17
  22.3 28.4 %all-to-all-done.1 = bf16[64,32,256]{2,1,0:T(8,128)(2,1)S(1)} async-done(((bf16[64,32,256]{2,1,0:T(8,128)(2,1)}), bf16[64,32,256]{2,1,0:T(8,128)(2,1)S(1)}, u32[]{:S(2)}, u32[]{:S(2)}) %all-to-all-start.1) | async-done | bytes 1048608 | tf_op jit(solution)/shard_map/all_to_all | solution.py:17
  51.7 4.1 %all-to-all-start = ((bf16[4,256,512]{1,2,0:T(8,128)(2,1)}), bf16[4,256,512]{1,2,0:T(8,128)(2,1)S(1)}, u32[]{:S(2)}, u32[]{:S(2)}) async-start(bf16[4,256,512]{1,2,0:T(8,128)(2,1)} %broadcast_in_dim.20), calls=%async_computation | async-start | bytes 2097152 | tf_op jit(solution)/shard_map/all_to_all | solution.py:17
  56.5 4.2 %collective-permute-start.4 = (bf16[2,16,128]{2,1,0:T(8,128)(2,1)S(1)}, bf16[2,16,128]{2,1,0:T(8,128)(2,1)S(1)}, u32[]{:S(2)}, u32[]{:S(2)}) collective-permute-start(bf16[2,16,128]{2,1,0:T(8,128)(2,1)S(1)} %get-tuple-element.23), channel_id=1, source_target_pairs={{0,4},{1,132},{2,260},{3,388},{4,0},{5,128},{6,256},{7,384},{64,68... | collective-permute-start | bytes 24584 | tf_op jit(solution)/shard_map/ppermute | solution.py:38
  60.8 1.9 collective-permute-start.1
  62.8 5.9 %all-to-all-done = bf16[4,256,512]{1,2,0:T(8,128)(2,1)S(1)} async-done(((bf16[4,256,512]{1,2,0:T(8,128)(2,1)}), bf16[4,256,512]{1,2,0:T(8,128)(2,1)S(1)}, u32[]{:S(2)}, u32[]{:S(2)}) %all-to-all-start) | async-done | bytes 1048608 | tf_op jit(solution)/shard_map/all_to_all | solution.py:17
  71.6 5.7 %collective-permute-start.2 = (bf16[128,256]{1,0:T(8,128)(2,1)S(1)}, bf16[128,256]{1,0:T(8,128)(2,1)S(1)}, u32[]{:S(2)}, u32[]{:S(2)}) collective-permute-start(bf16[128,256]{1,0:T(8,128)(2,1)S(1)} %slice.146), channel_id=1, source_target_pairs={{0,4},{4,8},{8,12},{12,16},{16,20},{20,24},{24,28},{28,32},{32,36}... | collective-permute-start | bytes 196616 | tf_op jit(solution)/shard_map/ppermute | solution.py:80
  78.2 13.4 %all-to-all-start.3 = ((bf16[64,32,128]{2,1,0:T(8,128)(2,1)}), bf16[64,32,128]{2,1,0:T(8,128)(2,1)S(1)}, u32[]{:S(2)}, u32[]{:S(2)}) async-start(bf16[64,32,128]{2,1,0:T(8,128)(2,1)} %broadcast_in_dim.46), calls=%async_computation.3 | async-start | bytes 1048576 | tf_op jit(solution)/shard_map/all_to_all | solution.py:17
  91.7 4.8 %fusion.47 = (f32[256]{0:T(256)S(1)}, f32[1,256,256]{2,0,1:T(1,128)S(1)}) fusion(f32[1,128,256]{2,1,0:T(8,128)S(1)} %get-tuple-element.12, bf16[1,383,256]{2,1,0:T(8,128)(2,1)S(1)} %maximum_bitcast_fusion), kind=kOutput, calls=%fused_computation.122 | convolution fusion | flops 100728576 | bytes 590336 | tf_op jit(solution)/shard_map/conv_general_dilated | solution.py:82
  96.8 13.4 %all-to-all-done.3 = bf16[64,32,128]{2,1,0:T(8,128)(2,1)S(1)} async-done(((bf16[64,32,128]{2,1,0:T(8,128)(2,1)}), bf16[64,32,128]{2,1,0:T(8,128)(2,1)S(1)}, u32[]{:S(2)}, u32[]{:S(2)}) %all-to-all-start.3) | async-done | bytes 524320 | tf_op jit(solution)/shard_map/all_to_all | solution.py:17
  110.3 10.5 %all_to_all.40 = bf16[4,272,256]{2,1,0:T(8,128)(2,1)S(1)} all-to-all(bf16[4,272,256]{2,1,0:T(8,128)(2,1)S(1)} %broadcast_in_dim.45), channel_id=1, replica_groups=mesh['z'=8,'y'=8,'c'=2,'x'=4] {'x'}, dimensions={0} | all-to-all | bytes 1114112 | tf_op jit(solution)/shard_map/all_to_all | solution.py:17
  121.9 6.8 %all-to-all-start.5 = ((bf16[64,32,256]{2,1,0:T(8,128)(2,1)}), bf16[64,32,256]{2,1,0:T(8,128)(2,1)S(1)}, u32[]{:S(2)}, u32[]{:S(2)}) async-start(bf16[64,32,256]{2,1,0:T(8,128)(2,1)} %broadcast_in_dim.48), calls=%async_computation.5 | async-start | bytes 2097152 | tf_op jit(solution)/shard_map/all_to_all | solution.py:17
  128.6 4.4 %collective-permute-start.5 = (bf16[4,512,128]{2,1,0:T(8,128)(2,1)S(1)}, bf16[4,512,128]{2,1,0:T(8,128)(2,1)S(1)}, u32[]{:S(2)}, u32[]{:S(2)}) collective-permute-start(bf16[4,512,128]{2,1,0:T(8,128)(2,1)S(1)} %bitcast.91), channel_id=1, source_target_pairs={{0,4},{4,0},{1,5},{5,1},{2,6},{6,2},{3,7},{7,3},{8,12},{12,8},{9,1... | collective-permute-start | bytes 1572872 | tf_op jit(solution)/shard_map/ppermute | solution.py:21
  135.0 20.3 %all-to-all-done.5 = bf16[64,32,256]{2,1,0:T(8,128)(2,1)S(1)} async-done(((bf16[64,32,256]{2,1,0:T(8,128)(2,1)}), bf16[64,32,256]{2,1,0:T(8,128)(2,1)S(1)}, u32[]{:S(2)}, u32[]{:S(2)}) %all-to-all-start.5) | async-done | bytes 1048608 | tf_op jit(solution)/shard_map/all_to_all | solution.py:17
  156.4 3.5 %all-to-all-start.4 = ((bf16[4,256,512]{1,2,0:T(8,128)(2,1)}), bf16[4,256,512]{1,2,0:T(8,128)(2,1)S(1)}, u32[]{:S(2)}, u32[]{:S(2)}) async-start(bf16[4,256,512]{1,2,0:T(8,128)(2,1)} %broadcast_in_dim.47), calls=%async_computation.4 | async-start | bytes 2097152 | tf_op jit(solution)/shard_map/all_to_all | solution.py:17
  159.9 6.1 %collective-permute-start.6 = (bf16[2048,256]{1,0:T(8,128)(2,1)S(1)}, bf16[2048,256]{1,0:T(8,128)(2,1)}, u32[]{:S(2)}, u32[]{:S(2)}) collective-permute-start(bf16[2048,256]{1,0:T(8,128)(2,1)S(1)} %bitcast.83), channel_id=1, source_target_pairs={{0,4},{4,0},{1,5},{5,1},{2,6},{6,2},{3,7},{7,3},{8,12},{12,8},{9,1... | collective-permute-start | bytes 3145736 | tf_op jit(solution)/shard_map/ppermute | solution.py:21
  166.1 4.5 %all-to-all-done.4 = bf16[4,256,512]{1,2,0:T(8,128)(2,1)S(1)} async-done(((bf16[4,256,512]{1,2,0:T(8,128)(2,1)}), bf16[4,256,512]{1,2,0:T(8,128)(2,1)S(1)}, u32[]{:S(2)}, u32[]{:S(2)}) %all-to-all-start.4) | async-done | bytes 1048608 | tf_op jit(solution)/shard_map/all_to_all | solution.py:17
  173.5 7.9 %collective-permute-start.7 = (bf16[128,256]{1,0:T(8,128)(2,1)S(1)}, bf16[128,256]{1,0:T(8,128)(2,1)S(1)}, u32[]{:S(2)}, u32[]{:S(2)}) collective-permute-start(bf16[128,256]{1,0:T(8,128)(2,1)S(1)} %slice.162), channel_id=1, source_target_pairs={{0,4},{4,8},{8,12},{12,16},{16,20},{20,24},{24,28},{28,32},{32,36}... | collective-permute-start | bytes 196616 | tf_op jit(solution)/shard_map/ppermute | solution.py:80
  182.3 8.0 %all-to-all-start.7 = ((bf16[64,32,128]{2,1,0:T(8,128)(2,1)}), bf16[64,32,128]{2,1,0:T(8,128)(2,1)S(1)}, u32[]{:S(2)}, u32[]{:S(2)}) async-start(bf16[64,32,128]{2,1,0:T(8,128)(2,1)} %broadcast_in_dim.51), calls=%async_computation.7 | async-start | bytes 1048576 | tf_op jit(solution)/shard_map/all_to_all | solution.py:17
  190.4 4.8 %fusion.48 = (f32[256]{0:T(256)S(1)}, f32[1,256,256]{2,0,1:T(1,128)S(1)}) fusion(f32[1,128,256]{2,1,0:T(8,128)S(1)} %get-tuple-element.11, bf16[1,383,256]{2,1,0:T(8,128)(2,1)S(1)} %maximum_bitcast_fusion.1), kind=kOutput, calls=%fused_computation.123 | convolution fusion | flops 100728576 | bytes 590336 | tf_op jit(solution)/shard_map/conv_general_dilated | solution.py:82
  195.5 14.0 %all-to-all-done.7 = bf16[64,32,128]{2,1,0:T(8,128)(2,1)S(1)} async-done(((bf16[64,32,128]{2,1,0:T(8,128)(2,1)}), bf16[64,32,128]{2,1,0:T(8,128)(2,1)S(1)}, u32[]{:S(2)}, u32[]{:S(2)}) %all-to-all-start.7) | async-done | bytes 524320 | tf_op jit(solution)/shard_map/all_to_all | solution.py:17
  210.3 3.5 %all-to-all-start.6 = ((bf16[4,272,256]{2,1,0:T(8,128)(2,1)}), bf16[4,272,256]{2,1,0:T(8,128)(2,1)S(1)}, u32[]{:S(2)}, u32[]{:S(2)}) async-start(bf16[4,272,256]{2,1,0:T(8,128)(2,1)} %broadcast_in_dim.50), calls=%async_computation.6 | async-start | bytes 1114112 | tf_op jit(solution)/shard_map/all_to_all | solution.py:17
  215.7 8.3 %all-to-all-done.6 = bf16[4,272,256]{2,1,0:T(8,128)(2,1)S(1)} async-done(((bf16[4,272,256]{2,1,0:T(8,128)(2,1)}), bf16[4,272,256]{2,1,0:T(8,128)(2,1)S(1)}, u32[]{:S(2)}, u32[]{:S(2)}) %all-to-all-start.6) | async-done | bytes 557088 | tf_op jit(solution)/shard_map/all_to_all | solution.py:17
  (86 shorter events, 22.5 us)
Async XLA Ops:
  0.7 3.4 %collective-permute-start = (bf16[2,16,256]{2,1,0:T(8,128)(2,1)S(1)}, bf16[2,16,256]{2,1,0:T(8,128)(2,1)S(1)}, u32[]{:S(2)}, u32[]{:S(2)}) collective-permute-start(bf16[2,16,256]{2,1,0:T(8,128)(2,1)S(1)} %broadcast_select_fusion.2), channel_id=1, source_target_pairs={{0,4},{4,0},{1,5},{5,1},{2,6},{6,2},{3,7},{7,3},{8,12},{12,8},{9,1... | collective-permute-start | bytes 49160 | tf_op jit(solution)/shard_map/ppermute | solution.py:21
  6.0 16.2 %copy-start = (bf16[256,512]{1,0:T(8,128)(2,1)S(1)}, bf16[256,512]{1,0:T(8,128)(2,1)}, u32[]{:S(2)}) copy-start(bf16[256,512]{1,0:T(8,128)(2,1)} %param.7) | copy-start | bytes 786436
  6.0 44.7 %all-to-all-start.1 = ((bf16[64,32,256]{2,1,0:T(8,128)(2,1)}), bf16[64,32,256]{2,1,0:T(8,128)(2,1)S(1)}, u32[]{:S(2)}, u32[]{:S(2)}) async-start(bf16[64,32,256]{2,1,0:T(8,128)(2,1)} %broadcast_in_dim.21), calls=%async_computation.1 | async-start | bytes 2097152 | tf_op jit(solution)/shard_map/all_to_all | solution.py:17
  51.7 4.2 %copy-start.2 = (bf16[2,256,16]{1,2,0:T(8,128)(2,1)S(1)}, bf16[2,256,16]{1,2,0:T(8,128)(2,1)}, u32[]{:S(2)}) copy-start(bf16[2,256,16]{1,2,0:T(8,128)(2,1)} %param.13) | copy-start | bytes 49156
  51.7 9.1 %copy-start.1 = (f32[2,128,256]{2,1,0:T(8,128)S(1)}, f32[2,128,256]{2,1,0:T(8,128)}, u32[]{:S(2)}) copy-start(f32[2,128,256]{2,1,0:T(8,128)} %param.11) | copy-start | bytes 786436
  51.7 9.1 %copy-start.3 = (f32[2,2048]{1,0:T(2,128)S(1)}, f32[2,2048]{1,0:T(2,128)}, u32[]{:S(2)}) copy-start(f32[2,2048]{1,0:T(2,128)} %param.8) | copy-start | bytes 49156
  51.7 17.0 %all-to-all-start = ((bf16[4,256,512]{1,2,0:T(8,128)(2,1)}), bf16[4,256,512]{1,2,0:T(8,128)(2,1)S(1)}, u32[]{:S(2)}, u32[]{:S(2)}) async-start(bf16[4,256,512]{1,2,0:T(8,128)(2,1)} %broadcast_in_dim.20), calls=%async_computation | async-start | bytes 2097152 | tf_op jit(solution)/shard_map/all_to_all | solution.py:17
  55.8 7.0 %collective-permute-start.3 = (bf16[2,16,128]{2,1,0:T(8,128)(2,1)S(1)}, bf16[2,16,128]{2,1,0:T(8,128)(2,1)S(1)}, u32[]{:S(2)}, u32[]{:S(2)}) collective-permute-start(bf16[2,16,128]{2,1,0:T(8,128)(2,1)S(1)} %get-tuple-element.24), channel_id=1, source_target_pairs={{0,0},{1,128},{2,256},{3,384},{4,4},{5,132},{6,260},{7,388},{64,64... | collective-permute-start | bytes 24584 | tf_op jit(solution)/shard_map/ppermute | solution.py:38
  56.5 6.3 %collective-permute-start.4 = (bf16[2,16,128]{2,1,0:T(8,128)(2,1)S(1)}, bf16[2,16,128]{2,1,0:T(8,128)(2,1)S(1)}, u32[]{:S(2)}, u32[]{:S(2)}) collective-permute-start(bf16[2,16,128]{2,1,0:T(8,128)(2,1)S(1)} %get-tuple-element.23), channel_id=1, source_target_pairs={{0,4},{1,132},{2,260},{3,388},{4,0},{5,128},{6,256},{7,384},{64,68... | collective-permute-start | bytes 24584 | tf_op jit(solution)/shard_map/ppermute | solution.py:38
  60.8 9.0 %collective-permute-start.1 = (bf16[2048,256]{1,0:T(8,128)(2,1)S(1)}, bf16[2048,256]{1,0:T(8,128)(2,1)}, u32[]{:S(2)}, u32[]{:S(2)}) collective-permute-start(bf16[2048,256]{1,0:T(8,128)(2,1)S(1)} %bitcast.85), channel_id=1, source_target_pairs={{0,4},{4,0},{1,5},{5,1},{2,6},{6,2},{3,7},{7,3},{8,12},{12,8},{9,1... | collective-permute-start | bytes 3145736 | tf_op jit(solution)/shard_map/ppermute | solution.py:21
  71.6 20.0 %collective-permute-start.2 = (bf16[128,256]{1,0:T(8,128)(2,1)S(1)}, bf16[128,256]{1,0:T(8,128)(2,1)S(1)}, u32[]{:S(2)}, u32[]{:S(2)}) collective-permute-start(bf16[128,256]{1,0:T(8,128)(2,1)S(1)} %slice.146), channel_id=1, source_target_pairs={{0,4},{4,8},{8,12},{12,16},{16,20},{20,24},{24,28},{28,32},{32,36}... | collective-permute-start | bytes 196616 | tf_op jit(solution)/shard_map/ppermute | solution.py:80
  78.2 32.0 %all-to-all-start.3 = ((bf16[64,32,128]{2,1,0:T(8,128)(2,1)}), bf16[64,32,128]{2,1,0:T(8,128)(2,1)S(1)}, u32[]{:S(2)}, u32[]{:S(2)}) async-start(bf16[64,32,128]{2,1,0:T(8,128)(2,1)} %broadcast_in_dim.46), calls=%async_computation.3 | async-start | bytes 1048576 | tf_op jit(solution)/shard_map/all_to_all | solution.py:17
  91.6 4.9 %copy-start.4 = (f32[2,256]{1,0:T(2,128)S(1)}, f32[2,256]{1,0:T(2,128)}, u32[]{:S(2)}) copy-start(f32[2,256]{1,0:T(2,128)} %param.12) | copy-start | bytes 6148
  121.9 33.5 %all-to-all-start.5 = ((bf16[64,32,256]{2,1,0:T(8,128)(2,1)}), bf16[64,32,256]{2,1,0:T(8,128)(2,1)S(1)}, u32[]{:S(2)}, u32[]{:S(2)}) async-start(bf16[64,32,256]{2,1,0:T(8,128)(2,1)} %broadcast_in_dim.48), calls=%async_computation.5 | async-start | bytes 2097152 | tf_op jit(solution)/shard_map/all_to_all | solution.py:17
  128.6 5.9 %collective-permute-start.5 = (bf16[4,512,128]{2,1,0:T(8,128)(2,1)S(1)}, bf16[4,512,128]{2,1,0:T(8,128)(2,1)S(1)}, u32[]{:S(2)}, u32[]{:S(2)}) collective-permute-start(bf16[4,512,128]{2,1,0:T(8,128)(2,1)S(1)} %bitcast.91), channel_id=1, source_target_pairs={{0,4},{4,0},{1,5},{5,1},{2,6},{6,2},{3,7},{7,3},{8,12},{12,8},{9,1... | collective-permute-start | bytes 1572872 | tf_op jit(solution)/shard_map/ppermute | solution.py:21
  156.4 14.2 %all-to-all-start.4 = ((bf16[4,256,512]{1,2,0:T(8,128)(2,1)}), bf16[4,256,512]{1,2,0:T(8,128)(2,1)S(1)}, u32[]{:S(2)}, u32[]{:S(2)}) async-start(bf16[4,256,512]{1,2,0:T(8,128)(2,1)} %broadcast_in_dim.47), calls=%async_computation.4 | async-start | bytes 2097152 | tf_op jit(solution)/shard_map/all_to_all | solution.py:17
  159.9 11.8 %collective-permute-start.6 = (bf16[2048,256]{1,0:T(8,128)(2,1)S(1)}, bf16[2048,256]{1,0:T(8,128)(2,1)}, u32[]{:S(2)}, u32[]{:S(2)}) collective-permute-start(bf16[2048,256]{1,0:T(8,128)(2,1)S(1)} %bitcast.83), channel_id=1, source_target_pairs={{0,4},{4,0},{1,5},{5,1},{2,6},{6,2},{3,7},{7,3},{8,12},{12,8},{9,1... | collective-permute-start | bytes 3145736 | tf_op jit(solution)/shard_map/ppermute | solution.py:21
  173.5 16.8 %collective-permute-start.7 = (bf16[128,256]{1,0:T(8,128)(2,1)S(1)}, bf16[128,256]{1,0:T(8,128)(2,1)S(1)}, u32[]{:S(2)}, u32[]{:S(2)}) collective-permute-start(bf16[128,256]{1,0:T(8,128)(2,1)S(1)} %slice.162), channel_id=1, source_target_pairs={{0,4},{4,8},{8,12},{12,16},{16,20},{20,24},{24,28},{28,32},{32,36}... | collective-permute-start | bytes 196616 | tf_op jit(solution)/shard_map/ppermute | solution.py:80
  182.3 27.2 %all-to-all-start.7 = ((bf16[64,32,128]{2,1,0:T(8,128)(2,1)}), bf16[64,32,128]{2,1,0:T(8,128)(2,1)S(1)}, u32[]{:S(2)}, u32[]{:S(2)}) async-start(bf16[64,32,128]{2,1,0:T(8,128)(2,1)} %broadcast_in_dim.51), calls=%async_computation.7 | async-start | bytes 1048576 | tf_op jit(solution)/shard_map/all_to_all | solution.py:17
  210.3 13.7 %all-to-all-start.6 = ((bf16[4,272,256]{2,1,0:T(8,128)(2,1)}), bf16[4,272,256]{2,1,0:T(8,128)(2,1)S(1)}, u32[]{:S(2)}, u32[]{:S(2)}) async-start(bf16[4,272,256]{2,1,0:T(8,128)(2,1)} %broadcast_in_dim.50), calls=%async_computation.6 | async-start | bytes 1114112 | tf_op jit(solution)/shard_map/all_to_all | solution.py:17
  213.8 11.4 %collective-permute-start.8 = (bf16[4,512,128]{2,1,0:T(8,128)(2,1)S(1)}, bf16[4,512,128]{2,1,0:T(8,128)(2,1)S(1)}, u32[]{:S(2)}, u32[]{:S(2)}) collective-permute-start(bf16[4,512,128]{2,1,0:T(8,128)(2,1)S(1)} %bitcast.93), channel_id=1, source_target_pairs={{0,4},{4,0},{1,5},{5,1},{2,6},{6,2},{3,7},{7,3},{8,12},{12,8},{9,1... | collective-permute-start | bytes 1572872 | tf_op jit(solution)/shard_map/ppermute | solution.py:21
